TPU v7x, 256 devices: a 4x2x16 block of a 4x16x16 slice. The times are simulated.
256 devices in a mesh: grp: 2 (over y), ep: 64 (over z, x), tp: 2 (over core).
Axes of the slice: x: 4, y: 2, z: 16, core: 2. Of those that a mesh axis runs over, the one named last changes fastest.
The devices are a block of a 4x16x16 slice.
Arguments:
- tokens: bfloat16 [32768, 2048], P(('grp', 'ep', 'tp')), parts along dimension 0, may hold values from -6 to 6
- norm_gain: float32 [2048], replicated, may hold values from 0.1 to 1.9
- expert_ids: int32 [32768, 2], P(('grp', 'ep', 'tp')), parts along dimension 0, may hold values from 0 to 31, all different within a row; in each aligned block of 128 rows (0 to 127, 128 to 255, ...) at most 10 rows name the same one
- route_weights: float32 [32768, 2], P(('grp', 'ep', 'tp')), parts along dimension 0, may hold values from 0.1 to 0.9
- w_gate: bfloat16 [2048, 114688], P(None, ('ep', 'tp')), may hold values from -0.125 to 0.125
- w_up: bfloat16 [2048, 114688], P(None, ('ep', 'tp')), may hold values from -0.125 to 0.125
- w_down: bfloat16 [114688, 2048], P(('ep', 'tp')), may hold values from -0.09375 to 0.09375
Outputs:
- mixed_out: bfloat16 [32768, 2048], P(('grp', 'ep', 'tp')), parts along dimension 0
There are 2 independent parts, one for each index of `grp`. A program takes and returns all parts, laid end to end along the dimension named above; an argument that names none is the same for every part. Nothing has to cross between parts.
Inputs may be any that keep to these rules, and one draw needn't show every extreme that they name: `expert_ids`: each row names 2 different experts. Among the rows of one device no expert is named more than 10 times, and in every draw some expert is named exactly 10 times by one device's rows.
All inputs are finite; a program needn't handle non-finite values.
Results may differ from a plain program's by a relative error of at most 0.01.
Values may be sent and summed in bfloat16 or wider, within the bound.
No kernel may reach another device: no remote copies, remote signals or barrier semaphores. Data moves between devices by JAX's collectives and lax.ppermute only.
A program may use at most 128 MiB of HBM per device.

v0:
```python
import jax
import jax.numpy as jnp
from jax import lax
from jax.sharding import PartitionSpec as P


def split_up(shard, dim, devices):
    before, after = (shard.shape[:dim], shard.shape[dim + 1 :])
    return jnp.moveaxis(shard.reshape(*before, devices, -1, *after), dim, 0)


def sum_at_owner(shard, axis, dim):
    devices = lax.axis_size(axis)
    blocks = lax.all_to_all(split_up(shard, dim, devices), axis, 0, 0, tiled=True)
    return jnp.sum(blocks.astype(jnp.float32), axis=0)


def partner_2(block, axis, apart):
    count = lax.axis_size(axis)
    route = []
    for low in range(count):
        high = low | 1 << apart
        if high != low and high < count:
            route += [(low, high), (high, low)]
    return lax.ppermute(block, axis, route)


def local(tokens, norm_gain, expert_ids, route_weights, w_gate, w_up, w_down):
    ep_count = lax.axis_size("ep")
    core_count = lax.axis_size("tp")
    expert_count = ep_count // 2
    tok_count = tokens.shape[0]
    model_width = tokens.shape[1]
    top_count = expert_ids.shape[1]
    capacity = 2 * max(1, 5 * tok_count * top_count // (8 * expert_count))
    source = lax.axis_index("ep") * core_count + lax.axis_index("tp")
    values = tokens.astype(jnp.float32)
    scale_rows = lax.rsqrt(jnp.mean(values * values, axis=1, keepdims=True) + 1e-06)
    normed = (values * scale_rows * norm_gain).astype(jnp.bfloat16)
    flat_ids = expert_ids.reshape(-1)
    route_count = flat_ids.shape[0]
    onehot = (flat_ids[:, None] == jnp.arange(expert_count, dtype=jnp.int32)[None, :]).astype(
        jnp.int32
    )
    earlier = jnp.cumsum(onehot, axis=0) - onehot
    slot_base = jnp.sum(earlier * onehot, axis=1)
    slot_index = jnp.remainder(slot_base + source, capacity)
    position = flat_ids * capacity + slot_index
    token_index = jnp.arange(route_count, dtype=jnp.int32) // top_count
    slot_table = (
        jnp.full((expert_count * capacity,), tok_count, jnp.int32).at[position].set(token_index)
    )
    padded = jnp.concatenate([normed, jnp.zeros((1, model_width), jnp.bfloat16)], axis=0)
    buffer = padded[slot_table].reshape(expert_count, capacity, model_width)
    half_slots = capacity // 2
    outgoing = buffer.reshape(ep_count, half_slots, model_width)
    arrived = lax.all_to_all(outgoing, "ep", split_axis=0, concat_axis=0, tiled=True).reshape(
        -1, model_width
    )
    partner = partner_2(arrived, "ep", 0)
    block_rows = lax.all_gather(
        jnp.concatenate([arrived, partner], axis=0), "tp", axis=0, tiled=True
    )
    gate_part = jnp.dot(block_rows, w_gate, preferred_element_type=jnp.float32)
    up_part = jnp.dot(block_rows, w_up, preferred_element_type=jnp.float32)
    hidden = (jax.nn.silu(gate_part) * up_part).astype(jnp.bfloat16)
    halves = sum_at_owner(
        jnp.dot(hidden, w_down, preferred_element_type=jnp.float32).astype(jnp.bfloat16), "tp", 0
    ).astype(jnp.bfloat16)
    own_rows = arrived.shape[0]
    partner_sums = partner_2(halves[own_rows:], "ep", 0)
    combined = (halves[:own_rows].astype(jnp.float32) + partner_sums.astype(jnp.float32)).astype(
        jnp.bfloat16
    )
    returned = lax.all_to_all(
        combined.reshape(ep_count, half_slots, model_width),
        "ep",
        split_axis=0,
        concat_axis=0,
        tiled=True,
    )
    summed = returned.reshape(expert_count, capacity, model_width).astype(jnp.float32)
    picked = summed.reshape(-1, model_width)[position].reshape(tok_count, top_count, model_width)
    mixed_out = jnp.sum(picked * route_weights[:, :, None], axis=1)
    return mixed_out.astype(jnp.bfloat16)


def solution(mesh):
    placed = (
        P(("grp", "ep", "tp"), None),
        P(),
        P(("grp", "ep", "tp"), None),
        P(("grp", "ep", "tp"), None),
        P(None, ("ep", "tp")),
        P(None, ("ep", "tp")),
        P(("ep", "tp"), None),
    )
    return jax.shard_map(
        local, mesh=mesh, in_specs=placed, out_specs=P(("grp", "ep", "tp"), None), check_vma=False
    )
```

profile of v0, /device:TPU:34, one launch (start us, length us, event | category | flops | bytes accessed | tf_op | source)
XLA Modules:
  0.0 411.0 jit_solution(868617568506192977)
XLA Ops:
  6.5 0.0 all-gather.2.cloned.1.call-start
  6.6 0.8 copy.10
  7.3 0.1 eq.31
  7.5 0.1 eq.27
  7.6 0.7 broadcast_multiply_fusion
  8.3 0.6 reduce-window.6
  8.9 0.2 slice_reduce_fusion
  9.1 0.1 copy.9
  9.3 0.1 mul.67
  9.4 0.1 fusion.6
  9.5 1.4 scatter_custom_fusion
  11.0 1.2 fusion.1
  12.2 1.2 fusion.3
  13.5 2.4 gather_fusion
  15.9 0.6 reshape_reshape.3
  16.5 127.6 %all_to_all.15 = bf16[64,5,2048]{2,1,0:T(8,128)(2,1)} all-to-all(bf16[64,5,2048]{2,1,0:T(8,128)(2,1)S(1)} %reshape_reshape.3), channel_id=1, replica_groups=mesh['grp'=2,'ep'=64,'tp'=2] {'ep'}, dimensions={0} | all-to-all | bytes 2621440 | tf_op jit(solution)/shard_map/all_to_all | solution.py:57
  144.1 2.6 reshape.99
  146.7 0.7 collective-permute-start
  147.4 26.9 %collective-permute-done = bf16[320,2048]{1,0:T(8,128)(2,1)S(1)} collective-permute-done((bf16[320,2048]{1,0:T(8,128)(2,1)S(1)}, bf16[320,2048]{1,0:T(8,128)(2,1)S(1)}, u32[]{:S(2)}, u32[]{:S(2)}) %collective-permute-start) | collective-permute-done | bytes 1310752 | tf_op jit(solution)/shard_map/ppermute | solution.py:25
  174.3 1.8 pad_maximum_fusion
  176.1 0.1 all-gather.2.cloned.1.call-update
  176.1 19.2 %all-gather.2.cloned.1.call-done = bf16[1280,2048]{1,0:T(8,128)(2,1)} async-done(((bf16[640,2048]{1,0:T(8,128)(2,1)}), bf16[1280,2048]{1,0:T(8,128)(2,1)}) %all-gather.2.cloned.1.call-update) | async-done | bytes 5242896 | tf_op jit(solution)/shard_map/all_gather | solution.py:61
  195.4 10.0 %fusion.14 = f32[1280,896]{1,0:T(8,128)} fusion(bf16[1280,2048]{1,0:T(8,128)(2,1)} %all-gather.2.cloned.1.call-done, bf16[2048,896]{1,0:T(8,128)(2,1)} %param.11), kind=kOutput, calls=%fused_computation.40 | convolution fusion | flops 4697620480 | bytes 13500416 | tf_op jit(solution)/shard_map/dot_general | solution.py:64
  205.4 17.6 %convolution_convert_fusion = bf16[1280,2048]{1,0:T(8,128)(2,1)} fusion(bf16[896,2048]{1,0:T(8,128)(2,1)} %param.13, f32[1280,896]{1,0:T(8,128)} %fusion.14, bf16[1280,2048]{1,0:T(8,128)(2,1)} %all-gather.2.cloned.1.call-done, bf16[2048,896]{1,0:T(8,128)(2,1)} %param.12), kind=kOutput, calls=%fused_computation.3 | convolution fusion | flops 9404743680 | bytes 22413312 | tf_op jit(solution)/shard_map/dot_general | solution.py:68
  222.9 13.8 %all_to_all.16 = bf16[2,640,2048]{2,1,0:T(8,128)(2,1)} all-to-all(bf16[2,640,2048]{2,1,0:T(8,128)(2,1)} %bitcast.27), channel_id=1, replica_groups=mesh['grp'=2,'ep'=64,'tp'=2] {'tp'}, dimensions={0} | all-to-all | bytes 10485760 | tf_op jit(solution)/shard_map/all_to_all | solution.py:14
  236.7 4.3 %reduce_sum.41 = bf16[640,2048]{1,0:T(8,128)(2,1)S(1)} reduce(bf16[2,640,2048]{2,1,0:T(8,128)(2,1)} %all_to_all.16, bf16[]{:T(256)} %constant.51.clone.1), dimensions={0}, to_apply=%region_5.6 | reduce | flops 1310720 | bytes 7864322 | tf_op jit(solution)/shard_map/reduce_sum | solution.py:15
  241.1 0.1 slice.22
  241.2 1.4 collective-permute-start.1
  242.5 29.6 %collective-permute-done.1 = bf16[320,2048]{1,0:T(8,128)(2,1)S(1)} collective-permute-done((bf16[320,2048]{1,0:T(8,128)(2,1)S(1)}, bf16[320,2048]{1,0:T(8,128)(2,1)S(1)}, u32[]{:S(2)}, u32[]{:S(2)}) %collective-permute-start.1) | collective-permute-done | bytes 1310752 | tf_op jit(solution)/shard_map/ppermute | solution.py:25
  272.1 1.5 add_convert_fusion
  273.6 0.0 copy-start
  273.6 3.4 reshape.101
  277.0 16.4 %all-to-all-start.2 = ((bf16[64,5,2048]{2,1,0:T(8,128)(2,1)}), bf16[64,5,2048]{2,1,0:T(8,128)(2,1)}, u32[]{:S(2)}, u32[]{:S(2)}) async-start(bf16[64,5,2048]{2,1,0:T(8,128)(2,1)} %reshape.101), calls=%async_computation.2 | async-start | bytes 4194304 | tf_op jit(solution)/shard_map/all_to_all | solution.py:75
  293.4 0.0 copy-done
  293.4 0.1 copy.13
  293.6 99.0 %all-to-all-done.2 = bf16[64,5,2048]{2,1,0:T(8,128)(2,1)} async-done(((bf16[64,5,2048]{2,1,0:T(8,128)(2,1)}), bf16[64,5,2048]{2,1,0:T(8,128)(2,1)}, u32[]{:S(2)}, u32[]{:S(2)}) %all-to-all-start.2) | async-done | bytes 1310752 | tf_op jit(solution)/shard_map/all_to_all | solution.py:75
  392.5 2.5 reshape.103
  395.0 2.7 gather_fusion.1
  397.7 2.5 reshape.102
  400.2 3.9 multiply_reduce_fusion
  (11 shorter events, 0.1 us)
Async XLA Ops:
  6.5 188.8 %all-gather.2.cloned.1.call-start = ((), (), s32[]{:S(2)}) async-start(), calls=%async_computation.3 | async-start | bytes 7864320 | tf_op jit(solution)/shard_map/all_gather | solution.py:61
  146.7 27.6 %collective-permute-start = (bf16[320,2048]{1,0:T(8,128)(2,1)S(1)}, bf16[320,2048]{1,0:T(8,128)(2,1)S(1)}, u32[]{:S(2)}, u32[]{:S(2)}) collective-permute-start(bf16[320,2048]{1,0:T(8,128)(2,1)S(1)} %reshape.99), channel_id=1, source_target_pairs={{0,2},{2,0},{4,6},{6,4},{8,10},{10,8},{12,14},{14,12},{16,18},{18,... | collective-permute-start | bytes 3932168 | tf_op jit(solution)/shard_map/ppermute | solution.py:25
  241.2 30.9 %collective-permute-start.1 = (bf16[320,2048]{1,0:T(8,128)(2,1)S(1)}, bf16[320,2048]{1,0:T(8,128)(2,1)S(1)}, u32[]{:S(2)}, u32[]{:S(2)}) collective-permute-start(bf16[320,2048]{1,0:T(8,128)(2,1)S(1)} %slice.22), channel_id=1, source_target_pairs={{0,2},{2,0},{4,6},{6,4},{8,10},{10,8},{12,14},{14,12},{16,18},{18,... | collective-permute-start | bytes 3932168 | tf_op jit(solution)/shard_map/ppermute | solution.py:25
  273.6 19.8 %copy-start = (f32[128,2]{0,1:T(2,128)S(1)}, f32[128,2]{0,1:T(2,128)}, u32[]{:S(2)}) copy-start(f32[128,2]{0,1:T(2,128)} %param.10) | copy-start | bytes 3076
  277.0 115.5 %all-to-all-start.2 = ((bf16[64,5,2048]{2,1,0:T(8,128)(2,1)}), bf16[64,5,2048]{2,1,0:T(8,128)(2,1)}, u32[]{:S(2)}, u32[]{:S(2)}) async-start(bf16[64,5,2048]{2,1,0:T(8,128)(2,1)} %reshape.101), calls=%async_computation.2 | async-start | bytes 4194304 | tf_op jit(solution)/shard_map/all_to_all | solution.py:75
Sparse Core Ops, SparseCore 0:
  176.3 19.0 all-gather.1
where the time goes:
time: 412 us; the launch traced here: 411 us
  waiting for transfers between devices  175 us (42%)
  blocking collectives  141 us (34%)
  matrix products  27.5 us (7%)
  local copies, waits for them, and re-layouts  19.8 us (5%)
  starting transfers between devices  18.4 us (4%)
  other arithmetic  15.5 us (4%)
  between operations  13.6 us (3%)
    all_to_all x1, blocking collectives, local(): lax.all_to_all(outgoing, 'ep', split_axis=0, concat_axis=0, tiled=True)  128 us
    all_to_all x1, waiting for transfers between devices, local(): lax.all_to_all(combined.reshape(ep_count, half_slots, model_width), 'ep',...  99 us
    ppermute x2, waiting for transfers between devices, partner_2(): return lax.ppermute(block, axis, route)  56.5 us
    all_gather x1, waiting for transfers between devices, local(): lax.all_gather(jnp.concatenate([arrived, partner], axis=0), 'tp', axis=0,...  19.2 us
    dot_general x1, matrix products, local(): jnp.dot(hidden, w_down, preferred_element_type=jnp.float32)  17.6 us
    all_to_all x1, starting transfers between devices, local(): lax.all_to_all(combined.reshape(ep_count, half_slots, model_width), 'ep',...  16.4 us
    all_to_all x1, blocking collectives, sum_at_owner(): lax.all_to_all(split_up(shard, dim, devices), axis, 0, 0, tiled=True)  13.8 us
    dot_general x1, matrix products, local(): gate_part = jnp.dot(block_rows, w_gate, preferred_element_type=jnp.float32)  9.98 us
  transfers between devices with their start and end apart: 4, of which 4 were waited for; matrix products, arithmetic and copies ran while one was open for 0% of the time, Pallas kernels for 0%

commit v1 on v0

--- a/solution.py
+++ b/solution.py
@@ -58,8 +58,14 @@
         -1, model_width
     )
     partner = partner_2(arrived, "ep", 0)
-    block_rows = lax.all_gather(
-        jnp.concatenate([arrived, partner], axis=0), "tp", axis=0, tiled=True
+    block_rows = jnp.concatenate(
+        lax.all_to_all(
+            jnp.stack([jnp.concatenate([arrived, partner], axis=0)] * lax.axis_size("tp")),
+            "tp",
+            0,
+            0,
+        ),
+        axis=0,
     )
     gate_part = jnp.dot(block_rows, w_gate, preferred_element_type=jnp.float32)
     up_part = jnp.dot(block_rows, w_up, preferred_element_type=jnp.float32)

time: 412 us -> 379 us (0.920)
  waiting for transfers between devices: 175 us -> 156 us
  between operations: 13.6 us -> 0.19 us
  blocking collectives: 141 us -> 149 us
  starting transfers between devices: 18.4 us -> 10.6 us
    all_gather x1 -> x0, waiting for transfers between devices: 19.2 us -> none  [local(): lax.all_gather(jnp.concatenate([arrived, partner], axis=0), 'tp', axis=0,...]
    all_to_all x0 -> x1, blocking collectives: none -> 8.23 us  [local(): lax.all_to_all(jnp.stack([jnp.concatenate([arrived, partner], axis=0)] *...]
    all_to_all x1, starting transfers between devices: 16.4 us -> 9.49 us  [local(): lax.all_to_all(combined.reshape(ep_count, half_slots, model_width), 'ep',...]
  transfers between devices with their start and end apart: 4 -> 3, of which waited for: 4 -> 3; matrix products, arithmetic and copies ran while one was open for 0% -> 0% of each run, Pallas kernels for 0% -> 0%
where the time goes in v1:
time: 379 us; the launch traced here: 378 us
  waiting for transfers between devices  156 us (41%)
  blocking collectives  149 us (39%)
  matrix products  24.7 us (7%)
  local copies, waits for them, and re-layouts  22.2 us (6%)
  other arithmetic  14.5 us (4%)
  starting transfers between devices  10.6 us (3%)
    all_to_all x1, blocking collectives, local(): lax.all_to_all(outgoing, 'ep', split_axis=0, concat_axis=0, tiled=True)  128 us
    all_to_all x1, waiting for transfers between devices, local(): lax.all_to_all(combined.reshape(ep_count, half_slots, model_width), 'ep',...  98.9 us
    ppermute x2, waiting for transfers between devices, partner_2(): return lax.ppermute(block, axis, route)  57.4 us
    dot_general x1, matrix products, local(): jnp.dot(hidden, w_down, preferred_element_type=jnp.float32)  17.5 us
    all_to_all x1, blocking collectives, sum_at_owner(): lax.all_to_all(split_up(shard, dim, devices), axis, 0, 0, tiled=True)  13.6 us
    all_to_all x1, starting transfers between devices, local(): lax.all_to_all(combined.reshape(ep_count, half_slots, model_width), 'ep',...  9.49 us
    all_to_all x1, blocking collectives, local(): lax.all_to_all(jnp.stack([jnp.concatenate([arrived, partner], axis=0)] *...  8.23 us
  transfers between devices with their start and end apart: 3, of which 3 were waited for; matrix products, arithmetic and copies ran while one was open for 0% of the time, Pallas kernels for 0%

profile of v1, /device:TPU:34, one launch (start us, length us, event | category | flops | bytes accessed | tf_op | source)
XLA Modules:
  0.0 377.9 jit_solution(17306708712699962949)
XLA Ops:
  0.0 0.8 copy.10
  0.8 0.1 eq.31
  0.9 0.1 eq.27
  1.1 0.7 broadcast_multiply_fusion
  1.8 0.6 reduce-window.6
  2.4 0.2 slice_reduce_fusion
  2.6 0.1 copy.9
  2.7 0.1 mul.67
  2.9 0.1 fusion.5
  3.0 1.4 scatter_custom_fusion
  4.4 1.2 fusion
  5.7 1.2 fusion.2
  6.9 2.4 gather_fusion
  9.4 0.6 reshape_reshape.3
  9.9 127.6 %all_to_all.20 = bf16[64,5,2048]{2,1,0:T(8,128)(2,1)} all-to-all(bf16[64,5,2048]{2,1,0:T(8,128)(2,1)S(1)} %reshape_reshape.3), channel_id=1, replica_groups=mesh['grp'=2,'ep'=64,'tp'=2] {'ep'}, dimensions={0} | all-to-all | bytes 2621440 | tf_op jit(solution)/shard_map/all_to_all | solution.py:57
  137.6 2.6 reshape.102
  140.2 0.7 collective-permute-start
  140.8 26.9 %collective-permute-done = bf16[320,2048]{1,0:T(8,128)(2,1)S(1)} collective-permute-done((bf16[320,2048]{1,0:T(8,128)(2,1)S(1)}, bf16[320,2048]{1,0:T(8,128)(2,1)S(1)}, u32[]{:S(2)}, u32[]{:S(2)}) %collective-permute-start) | collective-permute-done | bytes 1310752 | tf_op jit(solution)/shard_map/ppermute | solution.py:25
  167.7 0.3 maximum_bitcast_fusion
  168.1 0.5 pad_maximum_fusion
  168.5 0.0 copy-start.2
  168.5 8.2 %all_to_all.21 = bf16[2,640,2048]{2,1,0:T(8,128)(2,1)S(1)} all-to-all(bf16[2,640,2048]{2,1,0:T(8,128)(2,1)S(1)} %pad_maximum_fusion), channel_id=1, replica_groups=mesh['grp'=2,'ep'=64,'tp'=2] {'tp'}, dimensions={0} | all-to-all | bytes 10485760 | tf_op jit(solution)/shard_map/all_to_all | solution.py:62
  176.8 0.0 copy-start
  176.8 2.3 copy-done
  179.1 0.0 copy-done.2
  179.1 7.1 %fusion.11 = f32[1280,896]{1,0:T(8,128)} fusion(bf16[1280,2048]{1,0:T(8,128)(2,1)S(1)} %bitcast.30, bf16[2048,896]{1,0:T(8,128)(2,1)S(1)} %copy-done.2), kind=kOutput, calls=%fused_computation.39 | convolution fusion | flops 4697620480 | bytes 13500416 | tf_op jit(solution)/shard_map/dot_general | solution.py:70
  186.3 17.5 %convolution_convert_fusion = bf16[1280,2048]{1,0:T(8,128)(2,1)} fusion(bf16[896,2048]{1,0:T(8,128)(2,1)} %param.13, f32[1280,896]{1,0:T(8,128)} %fusion.11, bf16[1280,2048]{1,0:T(8,128)(2,1)} %bitcast.31, bf16[2048,896]{1,0:T(8,128)(2,1)} %param.12), kind=kOutput, calls=%fused_computation.3 | convolution fusion | flops 9404743680 | bytes 22413312 | tf_op jit(solution)/shard_map/dot_general | solution.py:74
  203.8 13.6 %all_to_all.22 = bf16[2,640,2048]{2,1,0:T(8,128)(2,1)} all-to-all(bf16[2,640,2048]{2,1,0:T(8,128)(2,1)} %bitcast.32), channel_id=1, replica_groups=mesh['grp'=2,'ep'=64,'tp'=2] {'tp'}, dimensions={0} | all-to-all | bytes 10485760 | tf_op jit(solution)/shard_map/all_to_all | solution.py:14
  217.4 4.3 %reduce_sum.41 = bf16[640,2048]{1,0:T(8,128)(2,1)S(1)} reduce(bf16[2,640,2048]{2,1,0:T(8,128)(2,1)} %all_to_all.22, bf16[]{:T(256)} %constant.51.clone.1), dimensions={0}, to_apply=%region_5.6 | reduce | flops 1310720 | bytes 7864322 | tf_op jit(solution)/shard_map/reduce_sum | solution.py:15
  221.7 0.1 slice.22
  221.8 0.4 collective-permute-start.1
  222.3 30.5 %collective-permute-done.1 = bf16[320,2048]{1,0:T(8,128)(2,1)S(1)} collective-permute-done((bf16[320,2048]{1,0:T(8,128)(2,1)S(1)}, bf16[320,2048]{1,0:T(8,128)(2,1)S(1)}, u32[]{:S(2)}, u32[]{:S(2)}) %collective-permute-start.1) | collective-permute-done | bytes 1310752 | tf_op jit(solution)/shard_map/ppermute | solution.py:25
  252.8 1.5 add_convert_fusion
  254.3 0.0 copy-start.1
  254.3 3.4 reshape.105
  257.7 9.5 %all-to-all-start.3 = ((bf16[64,5,2048]{2,1,0:T(8,128)(2,1)}), bf16[64,5,2048]{2,1,0:T(8,128)(2,1)}, u32[]{:S(2)}, u32[]{:S(2)}) async-start(bf16[64,5,2048]{2,1,0:T(8,128)(2,1)} %reshape.105), calls=%async_computation.3 | async-start | bytes 4194304 | tf_op jit(solution)/shard_map/all_to_all | solution.py:81
  267.2 0.0 copy-done.1
  267.2 0.1 copy.13
  267.3 98.9 %all-to-all-done.3 = bf16[64,5,2048]{2,1,0:T(8,128)(2,1)} async-done(((bf16[64,5,2048]{2,1,0:T(8,128)(2,1)}), bf16[64,5,2048]{2,1,0:T(8,128)(2,1)}, u32[]{:S(2)}, u32[]{:S(2)}) %all-to-all-start.3) | async-done | bytes 1310752 | tf_op jit(solution)/shard_map/all_to_all | solution.py:81
  366.3 2.5 reshape.107
  368.8 2.7 gather_fusion.1
  371.5 2.5 reshape.106
  374.0 3.9 %multiply_reduce_fusion = bf16[128,2048]{1,0:T(8,128)(2,1)} fusion(f32[128,2,2048]{2,1,0:T(2,128)S(1)} %reshape.106, f32[128,2]{1,0:T(8,128)S(1)} %copy.13), kind=kLoop, calls=%fused_computation.8 | loop fusion | flops 786432 | bytes 2622464 | tf_op jit(solution)/shard_map/reduce_sum | solution.py:90
  (11 shorter events, 0.1 us)
Async XLA Ops:
  140.2 27.6 %collective-permute-start = (bf16[320,2048]{1,0:T(8,128)(2,1)S(1)}, bf16[320,2048]{1,0:T(8,128)(2,1)S(1)}, u32[]{:S(2)}, u32[]{:S(2)}) collective-permute-start(bf16[320,2048]{1,0:T(8,128)(2,1)S(1)} %reshape.102), channel_id=1, source_target_pairs={{0,2},{2,0},{4,6},{6,4},{8,10},{10,8},{12,14},{14,12},{16,18},{18,... | collective-permute-start | bytes 3932168 | tf_op jit(solution)/shard_map/ppermute | solution.py:25
  168.5 10.6 %copy-start.2 = (bf16[2048,896]{1,0:T(8,128)(2,1)S(1)}, bf16[2048,896]{1,0:T(8,128)(2,1)}, u32[]{:S(2)}) copy-start(bf16[2048,896]{1,0:T(8,128)(2,1)} %param.11) | copy-start | bytes 11010052
  176.8 2.3 copy-start
  221.8 30.9 %collective-permute-start.1 = (bf16[320,2048]{1,0:T(8,128)(2,1)S(1)}, bf16[320,2048]{1,0:T(8,128)(2,1)S(1)}, u32[]{:S(2)}, u32[]{:S(2)}) collective-permute-start(bf16[320,2048]{1,0:T(8,128)(2,1)S(1)} %slice.22), channel_id=1, source_target_pairs={{0,2},{2,0},{4,6},{6,4},{8,10},{10,8},{12,14},{14,12},{16,18},{18,... | collective-permute-start | bytes 3932168 | tf_op jit(solution)/shard_map/ppermute | solution.py:25
  254.3 12.9 %copy-start.1 = (f32[128,2]{0,1:T(2,128)S(1)}, f32[128,2]{0,1:T(2,128)}, u32[]{:S(2)}) copy-start(f32[128,2]{0,1:T(2,128)} %param.10) | copy-start | bytes 3076
  257.7 108.6 %all-to-all-start.3 = ((bf16[64,5,2048]{2,1,0:T(8,128)(2,1)}), bf16[64,5,2048]{2,1,0:T(8,128)(2,1)}, u32[]{:S(2)}, u32[]{:S(2)}) async-start(bf16[64,5,2048]{2,1,0:T(8,128)(2,1)} %reshape.105), calls=%async_computation.3 | async-start | bytes 4194304 | tf_op jit(solution)/shard_map/all_to_all | solution.py:81
